TPU v7x, 32 devices: a whole 2x2x4 slice. The times are simulated.
32 devices in a mesh: dp: 4 (over y, x), kv: 4 (over z), tp: 2 (over core).
Axes of the slice: x: 2, y: 2, z: 4, core: 2. Of those that a mesh axis runs over, the one named last changes fastest.
Arguments:
- tokens: bfloat16 [1024, 4096], P('dp', ('kv', 'tp')), may hold values from -53 to 53
- carried_state: float32 [1024, 16, 128, 128], P(('dp', 'kv', 'tp')), may hold values from -9 to 9
- first_gain: float32 [4096], replicated, may hold values from 0.1 to 1.9
- first_gate: bfloat16 [4096, 11264], P(None, ('kv', 'tp')), may hold values from -0.09375 to 0.09375
- first_up: bfloat16 [4096, 11264], P(None, ('kv', 'tp')), may hold values from -0.09375 to 0.09375
- first_down: bfloat16 [11264, 4096], P(('kv', 'tp')), may hold values from -0.078125 to 0.078125
- mix_gain: float32 [4096], replicated, may hold values from 0.1 to 1.9
- query_weight: bfloat16 [4096, 2048], P(('kv', 'tp')), may hold values from -0.09375 to 0.09375
- forget_weight: bfloat16 [4096, 2048], P(('kv', 'tp')), may hold values from -0.09375 to 0.09375
- input_weight: bfloat16 [4096, 2048], P(('kv', 'tp')), may hold values from -0.09375 to 0.09375
- outgate_weight: bfloat16 [4096, 2048], P(('kv', 'tp')), may hold values from -0.09375 to 0.09375
- forget_floor: float32 [2048], replicated, may hold values from 0.05 to 0.9
- head_gain: float32 [128], replicated, may hold values from 0.1 to 1.9
- output_weight: bfloat16 [2048, 4096], P(None, ('kv', 'tp')), may hold values from -0.125 to 0.125
- second_gain: float32 [4096], replicated, may hold values from 0.1 to 1.9
- second_gate: bfloat16 [4096, 11264], P(None, ('kv', 'tp')), may hold values from -0.09375 to 0.09375
- second_up: bfloat16 [4096, 11264], P(None, ('kv', 'tp')), may hold values from -0.09375 to 0.09375
- second_down: bfloat16 [11264, 4096], P(('kv', 'tp')), may hold values from -0.078125 to 0.078125
Outputs:
- layer_out: bfloat16 [1024, 4096], P('dp', ('kv', 'tp'))
- next_state: float32 [1024, 16, 128, 128], P(('dp', 'kv', 'tp'))
All inputs are finite; a program needn't handle non-finite values.
Results may differ from a plain program's by a relative error of at most 0.018.
Values may be sent and summed in bfloat16 or wider, within the bound.
A program may use at most 256 MiB of HBM per device.

v0:
```python
import jax
import jax.numpy as jnp
from jax import lax
from jax.sharding import PartitionSpec as P

epsilon = 1e-06


def fold_step(gain_vec, gate_weight, up_weight, block_cols):
    widened = block_cols.astype(jnp.float32)
    scaled = (widened * gain_vec).astype(jnp.bfloat16)
    gate_acc = jnp.dot(scaled, gate_weight, preferred_element_type=jnp.float32)
    up_acc = jnp.dot(scaled, up_weight, preferred_element_type=jnp.float32)
    squares = jnp.sum(widened * widened, axis=1)
    return (gate_acc, up_acc, squares)


def channel_terms(own_cols, totals, down_weight, own_index, full_width):
    gate_acc, up_acc, squares = totals
    row_scale = lax.rsqrt(squares / full_width + epsilon)[:, None]
    hidden = (jax.nn.silu(row_scale * gate_acc) * (row_scale * up_acc)).astype(jnp.bfloat16)
    branch_sum = 0.5 * jnp.dot(hidden, down_weight, preferred_element_type=jnp.float32)
    own_part = lax.dynamic_update_slice_in_dim(
        jnp.zeros_like(branch_sum), own_cols.astype(jnp.float32), own_index * own_cols.shape[1], 1
    )
    return branch_sum + own_part


def per_device(
    tokens,
    carried_state,
    first_gain,
    first_gate,
    first_up,
    first_down,
    mix_gain,
    query_weight,
    forget_weight,
    input_weight,
    outgate_weight,
    forget_floor,
    head_gain,
    output_weight,
    second_gain,
    second_gate,
    second_up,
    second_down,
):
    own_index = lax.axis_index(("kv", "tp"))
    group_size = lax.axis_size(("kv", "tp"))
    share_cols = tokens.shape[1]
    full_width = share_cols * group_size
    first_totals = fold_step(
        first_gain, first_gate, first_up, lax.all_gather(tokens, ("kv", "tp"), axis=1, tiled=True)
    )
    first_terms = channel_terms(tokens, first_totals, first_down, own_index, full_width)
    mixer_share = lax.psum_scatter(
        first_terms, ("kv", "tp"), scatter_dimension=1, tiled=True
    ).astype(jnp.bfloat16)
    widened = mixer_share.astype(jnp.float32)
    squares = lax.psum(jnp.sum(widened * widened, axis=1), ("kv", "tp"))
    share_wide = mixer_share.astype(jnp.float32)
    mix_scaled = (
        share_wide * lax.dynamic_slice_in_dim(mix_gain, own_index * share_cols, share_cols)
    ).astype(jnp.bfloat16)
    state_rows, head_count, key_size, value_size = carried_state.shape
    projected = lax.psum_scatter(
        jnp.concatenate(
            [
                jnp.dot(mix_scaled, weight_part, preferred_element_type=jnp.float32)
                for weight_part in (query_weight, forget_weight, input_weight, outgate_weight)
            ],
            axis=1,
        ).astype(jnp.bfloat16),
        ("kv", "tp"),
        scatter_dimension=0,
        tiled=True,
    ).astype(jnp.float32)
    own_squares = lax.dynamic_slice_in_dim(squares, own_index * state_rows, state_rows)
    projected = projected * lax.rsqrt(own_squares / full_width + epsilon)[:, None]
    key_width = head_count * key_size
    value_width = head_count * value_size
    query_act = projected[:, :key_width].reshape(state_rows, head_count, key_size)
    forget_pre = projected[:, key_width : 2 * key_width].reshape(state_rows, head_count, key_size)
    input_val = projected[:, 2 * key_width : 2 * key_width + value_width].reshape(
        state_rows, head_count, value_size
    )
    gate_pre = projected[:, 2 * key_width + value_width :].reshape(
        state_rows, head_count, value_size
    )
    floor_grid = forget_floor.reshape(head_count, key_size)
    forget = floor_grid + (1.0 - floor_grid) * jax.nn.sigmoid(forget_pre)
    next_state = (
        forget[..., None] * carried_state + (1.0 - forget)[..., None] * input_val[:, :, None, :]
    )
    readout = jnp.sum(next_state * jax.nn.silu(query_act)[..., None], axis=2)
    normed = (
        readout
        * lax.rsqrt(jnp.mean(readout * readout, axis=-1, keepdims=True) + epsilon)
        * head_gain
    )
    mixer_out = (
        (normed * jax.nn.silu(gate_pre)).reshape(state_rows, value_width).astype(jnp.bfloat16)
    )
    update = jnp.dot(
        lax.all_gather(mixer_out, ("kv", "tp"), axis=0, tiled=True),
        output_weight,
        preferred_element_type=jnp.float32,
    )
    middle = (share_wide + update).astype(jnp.bfloat16)
    second_totals = fold_step(
        second_gain,
        second_gate,
        second_up,
        lax.all_gather(middle, ("kv", "tp"), axis=1, tiled=True),
    )
    second_terms = channel_terms(middle, second_totals, second_down, own_index, full_width)
    layer_out = lax.psum_scatter(
        second_terms.astype(jnp.bfloat16), ("kv", "tp"), scatter_dimension=1, tiled=True
    )
    return (layer_out, next_state)


def solution(mesh):
    in_specs = (
        P("dp", ("kv", "tp")),
        P(("dp", "kv", "tp"), None, None, None),
        P(),
        P(None, ("kv", "tp")),
        P(None, ("kv", "tp")),
        P(("kv", "tp"), None),
        P(),
        P(("kv", "tp"), None),
        P(("kv", "tp"), None),
        P(("kv", "tp"), None),
        P(("kv", "tp"), None),
        P(),
        P(),
        P(None, ("kv", "tp")),
        P(),
        P(None, ("kv", "tp")),
        P(None, ("kv", "tp")),
        P(("kv", "tp"), None),
    )
    out_specs = (P("dp", ("kv", "tp")), P(("dp", "kv", "tp"), None, None, None))
    return jax.shard_map(
        per_device, mesh=mesh, in_specs=in_specs, out_specs=out_specs, check_vma=False
    )
```

profile of v0, /device:TPU:0, one launch (start us, length us, event | category | flops | bytes accessed | tf_op | source)
XLA Modules:
  0.0 344.0 jit_solution(2094205272251710448)
XLA Ops:
  7.2 0.7 all-gather.4.cloned.1.call-update
  8.0 33.5 %all-gather.4.cloned.1.call-done = bf16[256,4096]{1,0:T(8,128)(2,1)} async-done(((bf16[256,512]{1,0:T(8,128)(2,1)}), bf16[256,4096]{1,0:T(8,128)(2,1)}) %all-gather.4.cloned.1.call-update) | async-done | bytes 2097168 | tf_op jit(solution)/shard_map/all_gather | solution.py:54
  41.5 2.1 fusion
  43.6 9.5 %convolution_multiply_fusion.5 = f32[256,1408]{1,0:T(8,128)} fusion(bf16[4096,1408]{1,0:T(8,128)(2,1)} %param.21, bf16[256,4096]{1,0:T(8,128)(2,1)} %all-gather.4.cloned.1.call-done, f32[4096]{0:T(1024)} %param.20, f32[256]{0:T(256)S(1)} %add_rsqrt_fusion.2), kind=kOutput, calls=%fused_computation.18 | convolution fusion | flops 2956296192 | bytes 15090688 | tf_op jit(solution)/shard_map/dot_general | solution.py:12
  53.1 17.4 %convolution_multiply_fusion.1 = f32[256,4096]{1,0:T(8,128)} fusion(bf16[1408,4096]{1,0:T(8,128)(2,1)} %param.23, bf16[4096,1408]{1,0:T(8,128)(2,1)} %param.22, bf16[256,4096]{1,0:T(8,128)(2,1)} %all-gather.4.cloned.1.call-done, f32[4096]{0:T(1024)S(1)} %copy-done.10, f32[256,1408]{1,0:T(8,128)} %convolution_multiply_fusion.5, f32[256]{0:T(256)S(1)} %add_rsqrt_fusion.2), kind=kOutput, calls=%fused_computation.3 | convolution fusion | flops 5912297472 | bytes 30819328 | tf_op jit(solution)/shard_map/dot_general | solution.py:22
  70.5 1.9 add_dynamic-update-slice_fusion.1
  72.5 0.8 dynamic_slice.6
  73.2 48.7 %reduce-scatter.4.cloned.1.call-done = f32[256,512]{1,0:T(8,128)} async-done(((f32[256,4096]{1,0:T(8,128)}), f32[256,512]{1,0:T(8,128)}) %reduce-scatter.4.cloned.1.call-update) | async-done | bytes 524304 | tf_op jit(solution)/shard_map/reduce_scatter | solution.py:57
  121.9 1.3 fusion.18
  123.2 0.7 convolution_convert_fusion.1
  124.0 0.7 convolution_convert_fusion
  124.7 0.7 convolution_convert_fusion.2
  125.4 0.2 copy-done.4
  125.6 0.7 convolution_convert_fusion.3
  126.3 2.2 pad_maximum_fusion
  128.6 0.6 copy-done.9
  129.3 14.5 %psum.7 = f32[256]{0:T(256)S(1)} all-reduce(f32[256]{0:T(256)S(1)} %get-tuple-element.6), channel_id=1, replica_groups=mesh['dp'=4,'kv'=4,'tp'=2] {'kv','tp'}, use_global_device_ids=true, to_apply=%region_4.5 | all-reduce | flops 256 | bytes 2048 | tf_op jit(solution)/shard_map/psum | solution.py:61
  143.8 33.5 %reduce-scatter.6.cloned.1.call-done = bf16[32,8192]{1,0:T(8,128)(2,1)} async-done(((bf16[256,8192]{1,0:T(8,128)(2,1)}), bf16[32,8192]{1,0:T(8,128)(2,1)}) %reduce-scatter.6.cloned.1.call-update) | async-done | bytes 524304 | tf_op jit(solution)/shard_map/reduce_scatter | solution.py:67
  177.3 1.2 convert_multiply_fusion.4
  178.8 34.1 %multiply_reduce_fusion = (f32[32,16,128]{2,1,0:T(8,128)S(1)}, f32[32,16,128,128]{3,2,1,0:T(8,128)}) fusion(f32[32,16,128]{2,1,0:T(8,128)S(1)} %get-tuple-element.11, f32[32,16,128]{2,1,0:T(8,128)S(1)} %bitcast.46, f32[32,16,128]{2,1,0:T(8,128)S(1)} %get-tuple-element.4, f32[32,16,128,128]{3,2,1,0:T(8,128)} %param.19, f32[32,16,128]{2,1,0:T(8,128)S(1)} %get-tuple-element.5), kind=kLoop, calls=%fused_computation | loop fusion | flops 41877504 | bytes 68419584 | tf_op jit(solution)/shard_map/reduce_sum | solution.py:96
  212.9 0.1 multiply_reduce_fusion.1
  213.1 0.1 broadcast_multiply_fusion
  213.2 0.8 fusion.20
  214.0 20.8 %all-gather.6.cloned.1.call-done = bf16[256,2048]{1,0:T(8,128)(2,1)} async-done(((bf16[32,2048]{1,0:T(8,128)(2,1)}), bf16[256,2048]{1,0:T(8,128)(2,1)}) %all-gather.6.cloned.1.call-update) | async-done | bytes 1048592 | tf_op jit(solution)/shard_map/all_gather | solution.py:106
  234.9 3.3 fusion.12
  238.3 28.9 %all-gather.8.cloned.1.call-done = bf16[256,4096]{1,0:T(8,128)(2,1)} async-done(((bf16[256,512]{1,0:T(8,128)(2,1)}), bf16[256,4096]{1,0:T(8,128)(2,1)}) %all-gather.8.cloned.1.call-update) | async-done | bytes 2097168 | tf_op jit(solution)/shard_map/all_gather | solution.py:115
  267.1 2.1 fusion.2
  269.3 9.6 %convolution_multiply_fusion.3 = f32[256,1408]{1,0:T(8,128)} fusion(bf16[4096,1408]{1,0:T(8,128)(2,1)} %param.33, bf16[256,4096]{1,0:T(8,128)(2,1)} %all-gather.8.cloned.1.call-done, f32[4096]{0:T(1024)S(1)} %copy-done.11, f32[256]{0:T(256)S(1)} %add_rsqrt_fusion.1), kind=kOutput, calls=%fused_computation.15 | convolution fusion | flops 2956296192 | bytes 15090688 | tf_op jit(solution)/shard_map/dot_general | solution.py:12
  278.9 16.8 %convolution_multiply_fusion = f32[256,4096]{1,0:T(8,128)} fusion(bf16[1408,4096]{1,0:T(8,128)(2,1)} %param.35, bf16[4096,1408]{1,0:T(8,128)(2,1)} %param.34, bf16[256,4096]{1,0:T(8,128)(2,1)S(1)} %copy-done.5, f32[4096]{0:T(1024)S(1)} %copy-done.11, f32[256,1408]{1,0:T(8,128)} %convolution_multiply_fusion.3, f32[256]{0:T(256)S(1)} %add_rsqrt_fusion.1), kind=kOutput, calls=%fused_computation.2 | convolution fusion | flops 5912297472 | bytes 30819328 | tf_op jit(solution)/shard_map/dot_general | solution.py:22
  295.6 2.1 add_dynamic-update-slice_fusion
  297.8 3.8 %convert_element_type.61 = bf16[256,4096]{1,0:T(8,128)(2,1)} convert(f32[256,4096]{1,0:T(8,128)} %add_dynamic-update-slice_fusion) | non-fusion elementwise | flops 1048576 | bytes 6291456 | tf_op jit(solution)/shard_map/convert_element_type | solution.py:119
  301.6 35.6 %reduce-scatter.8.cloned.1.call-done = bf16[256,512]{1,0:T(8,128)(2,1)} async-done(((bf16[256,4096]{1,0:T(8,128)(2,1)}), bf16[256,512]{1,0:T(8,128)(2,1)}) %reduce-scatter.8.cloned.1.call-update) | async-done | bytes 262160 | tf_op jit(solution)/shard_map/reduce_scatter | solution.py:118
  (44 shorter events, 0.9 us)
Async XLA Ops:
  7.2 116.0 %copy-start = (bf16[512,2048]{1,0:T(8,128)(2,1)S(1)}, bf16[512,2048]{1,0:T(8,128)(2,1)}, u32[]{:S(2)}) copy-start(bf16[512,2048]{1,0:T(8,128)(2,1)} %param.27) | copy-start | bytes 6291460
  7.2 34.3 %all-gather.4.cloned.1.call-start = ((), (), s32[]{:S(2)}) async-start(), calls=%async_computation.3 | async-start | bytes 2359296 | tf_op jit(solution)/shard_map/all_gather | solution.py:54
  7.9 114.0 %reduce-scatter.4.cloned.1.call-start = ((), (), s32[]{:S(2)}) async-start(), calls=%async_computation.4 | async-start | bytes 4718592 | tf_op jit(solution)/shard_map/reduce_scatter | solution.py:57
  43.6 9.5 %copy-start.10 = (f32[4096]{0:T(1024)S(1)}, f32[4096]{0:T(1024)}, u32[]{:S(2)}) copy-start(f32[4096]{0:T(1024)} %param.20) | copy-start | bytes 49156
  53.1 17.4 %copy-start.6 = (bf16[256,512]{1,0:T(8,128)(2,1)S(1)}, bf16[256,512]{1,0:T(8,128)(2,1)}, u32[]{:S(2)}) copy-start(bf16[256,512]{1,0:T(8,128)(2,1)} %param.18) | copy-start | bytes 786436
  72.4 104.9 %reduce-scatter.6.cloned.1.call-start = ((), (), s32[]{:S(2)}) async-start(), calls=%async_computation.5 | async-start | bytes 4718592 | tf_op jit(solution)/shard_map/reduce_scatter | solution.py:67
  121.9 2.0 copy-start.2
  121.9 2.8 copy-start.3
  123.9 1.7 copy-start.4
  128.6 0.7 copy-start.9
  128.6 0.7 copy-start.8
  128.6 106.3 %all-gather.6.cloned.1.call-start = ((), (), s32[]{:S(2)}) async-start(), calls=%async_computation.6 | async-start | bytes 1179648 | tf_op jit(solution)/shard_map/all_gather | solution.py:106
  212.9 56.4 %copy-start.11 = (f32[4096]{0:T(1024)S(1)}, f32[4096]{0:T(1024)}, u32[]{:S(2)}) copy-start(f32[4096]{0:T(1024)} %param.32) | copy-start | bytes 49156
  214.0 53.2 %all-gather.8.cloned.1.call-start = ((), (), s32[]{:S(2)}) async-start(), calls=%async_computation.7 | async-start | bytes 2359296 | tf_op jit(solution)/shard_map/all_gather | solution.py:115
  238.2 98.9 %reduce-scatter.8.cloned.1.call-start = ((), (), s32[]{:S(2)}) async-start(), calls=%async_computation.8 | async-start | bytes 2359296 | tf_op jit(solution)/shard_map/reduce_scatter | solution.py:118
  269.2 9.6 %copy-start.5 = (bf16[256,4096]{1,0:T(8,128)(2,1)S(1)}, bf16[256,4096]{1,0:T(8,128)(2,1)}, u32[]{:S(2)}) copy-start(bf16[256,4096]{1,0:T(8,128)(2,1)} %all-gather.8.cloned.1.call-done) | copy-start | bytes 6291460
  278.9 16.8 %copy-start.7 = (bf16[256,512]{1,0:T(8,128)(2,1)S(1)}, bf16[256,512]{1,0:T(8,128)(2,1)}, u32[]{:S(2)}) copy-start(bf16[256,512]{1,0:T(8,128)(2,1)} %fusion.12) | copy-start | bytes 786436
  295.6 41.5 %copy-start.1 = (bf16[512,2048]{1,0:T(8,128)(2,1)S(1)}, bf16[512,2048]{1,0:T(8,128)(2,1)}, u32[]{:S(2)}) copy-start(bf16[512,2048]{1,0:T(8,128)(2,1)} %param.27) | copy-start | bytes 6291460
Sparse Core Ops, SparseCore 0:
  9.6 31.8 all-gather.3
  72.5 49.3 reduce-scatter.3
  128.7 48.5 reduce-scatter.5
  214.1 20.7 all-gather.5
  238.4 28.7 all-gather.7
  301.7 35.4 reduce-scatter.7
where the time goes:
time: 344 us
  waiting for transfers between devices  202 us (59%)
  matrix products  59.4 us (17%)
  other arithmetic  52.1 us (15%)
  blocking collectives  14.5 us (4%)
  between operations  14.3 us (4%)
    reduce_scatter x1, waiting for transfers between devices, per_device(): lax.psum_scatter(first_terms, ('kv', 'tp'), scatter_dimension=1, tiled=True)  48.7 us
    reduce_scatter x1, waiting for transfers between devices, per_device(): lax.psum_scatter(second_terms.astype(jnp.bfloat16), ('kv', 'tp'), scatter...  35.6 us
    dot_general x2, matrix products, channel_terms(): jnp.dot(hidden, down_weight, preferred_element_type=jnp.float32)  34.1 us
    reduce_sum x1, other arithmetic, per_device(): readout = jnp.sum(next_state * jax.nn.silu(query_act)[..., None], axis=2)  34.1 us
    all_gather x1, waiting for transfers between devices, per_device(): lax.all_gather(tokens, ('kv', 'tp'), axis=1, tiled=True)  33.5 us
    reduce_scatter x1, waiting for transfers between devices, per_device(): lax.psum_scatter(jnp.concatenate([jnp.dot(mix_scaled, weight_part, prefer...  33.5 us
    all_gather x1, waiting for transfers between devices, per_device(): lax.all_gather(middle, ('kv', 'tp'), axis=1, tiled=True)  28.9 us
    all_gather x1, waiting for transfers between devices, per_device(): lax.all_gather(mixer_out, ('kv', 'tp'), axis=0, tiled=True)  20.8 us
  transfers between devices with their start and end apart: 6, of which 6 were waited for; matrix products, arithmetic and copies ran while one was open for 0% of the time, Pallas kernels for 0%

commit v1 on v0

v1 whole, which is shorter than its diff:
```python
import functools

import jax
import jax.numpy as jnp
from jax import lax
from jax.experimental import pallas as pl
from jax.experimental.pallas import tpu as pltpu
from jax.sharding import PartitionSpec as P

epsilon = 1e-06
MESH = pl.DeviceIdType.MESH
VMEM_LIMIT = 62 * 1024 * 1024


def remote(src, dst, send_sem, recv_sem, kv, tp):
    return pltpu.make_async_remote_copy(
        src_ref=src,
        dst_ref=dst,
        send_sem=send_sem,
        recv_sem=recv_sem,
        device_id={"kv": kv, "tp": tp},
        device_id_type=MESH,
    )


def greet(me, core, chips):
    barrier = pltpu.get_barrier_semaphore()
    pl.semaphore_signal(
        barrier, inc=1, device_id={"kv": me, "tp": 1 - core}, device_id_type=MESH
    )
    for step in range(1, chips):
        pl.semaphore_signal(
            barrier,
            inc=1,
            device_id={"kv": lax.rem(me + step, chips), "tp": core},
            device_id_type=MESH,
        )
    pl.semaphore_wait(barrier, chips)


def gather_kernel(chips, own_ref, full_ref, local_sem, chip_send, sib_send, recv_sem):
    me = lax.axis_index("kv")
    core = lax.axis_index("tp")
    mine = me * 2 + core
    local = pltpu.make_async_copy(own_ref, full_ref.at[mine], local_sem)
    local.start()
    greet(me, core, chips)
    sends = []
    for step in range(1, chips):
        peer = lax.rem(me + chips - step, chips)
        copy = remote(
            own_ref, full_ref.at[mine], chip_send.at[step], recv_sem.at[mine], peer, core
        )
        copy.start()
        sends.append(copy)
    copy = remote(own_ref, full_ref.at[mine], sib_send.at[0], recv_sem.at[mine], me, 1 - core)
    copy.start()
    sends.append(copy)
    for step in range(1, chips):
        slot = lax.rem(me + step, chips) * 2 + core
        remote(
            full_ref.at[slot], full_ref.at[slot], chip_send.at[0], recv_sem.at[slot], me, 1 - core
        ).wait_recv()
        copy = remote(
            full_ref.at[slot], full_ref.at[slot], sib_send.at[step], recv_sem.at[slot], me, 1 - core
        )
        copy.start()
        sends.append(copy)
    for step in range(chips):
        slot = lax.rem(me + step, chips) * 2 + 1 - core
        remote(
            full_ref.at[slot], full_ref.at[slot], chip_send.at[0], recv_sem.at[slot], me, 1 - core
        ).wait_recv()
    for copy in sends:
        copy.wait_send()
    local.wait()


def gather_rows(own, chips, collective_id):
    blocks = chips * 2
    return pl.pallas_call(
        functools.partial(gather_kernel, chips),
        out_shape=jax.ShapeDtypeStruct((blocks,) + own.shape, own.dtype),
        in_specs=[pl.BlockSpec(memory_space=pltpu.VMEM)],
        out_specs=pl.BlockSpec(memory_space=pltpu.VMEM),
        scratch_shapes=[
            pltpu.SemaphoreType.DMA,
            pltpu.SemaphoreType.DMA((chips,)),
            pltpu.SemaphoreType.DMA((chips,)),
            pltpu.SemaphoreType.DMA((blocks,)),
        ],
        compiler_params=pltpu.CompilerParams(
            collective_id=collective_id, has_side_effects=True, vmem_limit_bytes=VMEM_LIMIT
        ),
    )(own)


def block_kernel(
    chips,
    own_ref,
    gain_ref,
    gate_hbm,
    up_hbm,
    down_hbm,
    out_ref,
    gate_w,
    up_w,
    down_w,
    cols,
    gate_acc,
    up_acc,
    squares,
    hidden,
    sib_out,
    sib_in,
    chip_out,
    chip_in,
    gate_sem,
    up_sem,
    down_sem,
    local_sem,
    chip_send,
    sib_send,
    recv_sem,
    sib_out_sem,
    sib_in_sem,
    chip_out_sem,
    chip_in_sem,
):
    me = lax.axis_index("kv")
    core = lax.axis_index("tp")
    mine = me * 2 + core
    rows, width = own_ref.shape
    full_width = width * chips * 2

    def gate_copy(j):
        at = pl.ds(pl.multiple_of(j * width, width), width)
        return pltpu.make_async_copy(gate_hbm.at[at, :], gate_w.at[j], gate_sem.at[j])

    def up_copy(j):
        at = pl.ds(pl.multiple_of(j * width, width), width)
        return pltpu.make_async_copy(up_hbm.at[at, :], up_w.at[j], up_sem.at[j])

    def down_copy(j):
        at = pl.ds(pl.multiple_of(j * width, width), width)
        return pltpu.make_async_copy(down_hbm.at[:, at], down_w.at[j], down_sem.at[j])

    local = pltpu.make_async_copy(own_ref, cols.at[mine], local_sem)
    local.start()

    @pl.loop(0, chips)
    def _(step):
        q = lax.rem(me + step, chips)
        for c in (core, 1 - core):
            gate_copy(q * 2 + c).start()
            up_copy(q * 2 + c).start()

    greet(me, core, chips)

    def share_copy(step):
        return remote(
            own_ref,
            cols.at[mine],
            chip_send.at[step],
            recv_sem.at[mine],
            lax.rem(me + chips - step, chips),
            core,
        )

    def pass_copy(slot, step):
        return remote(
            cols.at[slot], cols.at[slot], sib_send.at[step], recv_sem.at[slot], me, 1 - core
        )

    @pl.loop(1, chips)
    def _(step):
        share_copy(step).start()

    @pl.loop(0, chips)
    def _(step):
        q = lax.rem(me + 1 + step, chips)
        for c in (1 - core, core):
            down_copy(q * 2 + c).start()

    gate_acc[...] = jnp.zeros_like(gate_acc)
    up_acc[...] = jnp.zeros_like(up_acc)
    squares[...] = jnp.zeros_like(squares)
    local.wait()

    def take(j):
        block = cols[j].astype(jnp.float32)
        squares[...] += jnp.sum(block * block, axis=1, keepdims=True)
        scaled = (block * gain_ref[j]).astype(jnp.bfloat16)
        gate_copy(j).wait()
        gate_acc[...] += jnp.dot(scaled, gate_w[j], preferred_element_type=jnp.float32)
        up_copy(j).wait()
        up_acc[...] += jnp.dot(scaled, up_w[j], preferred_element_type=jnp.float32)

    @pl.loop(0, chips * 2)
    def _(turn):
        step = lax.div(turn, 2)
        other = lax.rem(turn, 2)
        q = lax.rem(me + step, chips)
        slot = q * 2 + lax.rem(core + other, 2)

        @pl.when(turn > 0)
        def _():
            pass_copy(slot, step).wait_recv()

        @pl.when(other == 0)
        def _():
            pass_copy(slot, step).start()

        take(slot)

    tile = 32

    @pl.loop(0, rows // tile)
    def _(i):
        at = pl.ds(pl.multiple_of(i * tile, tile), tile)
        row_scale = lax.rsqrt(squares[at, :] / full_width + epsilon)
        gate = row_scale * gate_acc[at, :]
        hidden[at, :] = (gate * jax.nn.sigmoid(gate) * (row_scale * up_acc[at, :])).astype(
            jnp.bfloat16
        )

    def branch(j):
        down_copy(j).wait()
        return 0.5 * jnp.dot(hidden[...], down_w[j], preferred_element_type=jnp.float32)

    def sib_copy(q):
        return remote(
            sib_out.at[q], sib_in.at[q], sib_out_sem.at[q], sib_in_sem.at[q], me, 1 - core
        )

    def chip_copy(q):
        return remote(
            chip_out.at[q], chip_in.at[me], chip_out_sem.at[q], chip_in_sem.at[me], q, core
        )

    @pl.loop(0, chips)
    def _(step):
        q = lax.rem(me + 1 + step, chips)
        sib_out[q] = branch(q * 2 + 1 - core).astype(jnp.bfloat16)
        sib_copy(q).start()
        part = branch(q * 2 + core)
        sib_copy(q).wait_recv()
        chip_out[q] = (part + sib_in[q].astype(jnp.float32)).astype(jnp.bfloat16)

        @pl.when(step < chips - 1)
        def _():
            chip_copy(q).start()

        @pl.when(step == chips - 1)
        def _():
            gate_acc[:, :width] = part + sib_in[q].astype(jnp.float32)

    total = gate_acc[:, :width] + own_ref[...].astype(jnp.float32)
    for step in range(1, chips):
        q = lax.rem(me + step, chips)
        remote(
            chip_out.at[q], chip_in.at[q], chip_out_sem.at[q], chip_in_sem.at[q], q, core
        ).wait_recv()
        total = total + chip_in[q].astype(jnp.float32)
    out_ref[...] = total.astype(out_ref.dtype)

    @pl.loop(0, chips)
    def _(step):
        slot = lax.rem(me + step, chips) * 2 + core
        pass_copy(slot, step).wait_send()
        sib_copy(step).wait_send()

    @pl.loop(1, chips)
    def _(step):
        share_copy(step).wait_send()
        chip_copy(lax.rem(me + step, chips)).wait_send()


def feed_forward(own, gain, gate, up, down, chips, collective_id):
    rows, width = own.shape
    units = gate.shape[1]
    blocks = chips * 2
    dma = pltpu.SemaphoreType.DMA
    acc_width = max(units, width)
    return pl.pallas_call(
        functools.partial(block_kernel, chips),
        out_shape=jax.ShapeDtypeStruct((rows, width), jnp.bfloat16),
        in_specs=[pl.BlockSpec(memory_space=pltpu.VMEM)] * 2
        + [pl.BlockSpec(memory_space=pl.ANY)] * 3,
        out_specs=pl.BlockSpec(memory_space=pltpu.VMEM),
        scratch_shapes=[
            pltpu.VMEM((blocks, width, units), jnp.bfloat16),
            pltpu.VMEM((blocks, width, units), jnp.bfloat16),
            pltpu.VMEM((blocks, units, width), jnp.bfloat16),
            pltpu.VMEM((blocks, rows, width), jnp.bfloat16),
            pltpu.VMEM((rows, units), jnp.float32),
            pltpu.VMEM((rows, units), jnp.float32),
            pltpu.VMEM((rows, 1), jnp.float32),
            pltpu.VMEM((rows, units), jnp.bfloat16),
            pltpu.VMEM((chips, rows, width), jnp.bfloat16),
            pltpu.VMEM((chips, rows, width), jnp.bfloat16),
            pltpu.VMEM((chips, rows, width), jnp.bfloat16),
            pltpu.VMEM((chips, rows, width), jnp.bfloat16),
            dma((blocks,)),
            dma((blocks,)),
            dma((blocks,)),
            dma,
            dma((chips,)),
            dma((chips,)),
            dma((blocks,)),
            dma((chips,)),
            dma((chips,)),
            dma((chips,)),
            dma((chips,)),
        ],
        compiler_params=pltpu.CompilerParams(
            collective_id=collective_id, has_side_effects=True, vmem_limit_bytes=VMEM_LIMIT
        ),
    )(own, gain.reshape(blocks, 1, width), gate, up, down)


def per_device(
    tokens,
    carried_state,
    first_gain,
    first_gate,
    first_up,
    first_down,
    mix_gain,
    query_weight,
    forget_weight,
    input_weight,
    outgate_weight,
    forget_floor,
    head_gain,
    output_weight,
    second_gain,
    second_gate,
    second_up,
    second_down,
):
    own_index = lax.axis_index(("kv", "tp"))
    group_size = lax.axis_size(("kv", "tp"))
    share_cols = tokens.shape[1]
    full_width = share_cols * group_size
    chips = lax.axis_size("kv")
    mixer_share = feed_forward(tokens, first_gain, first_gate, first_up, first_down, chips, 0)
    share_wide = mixer_share.astype(jnp.float32)
    mix_scaled = (
        share_wide * lax.dynamic_slice_in_dim(mix_gain, own_index * share_cols, share_cols)
    ).astype(jnp.bfloat16)
    state_rows, head_count, key_size, value_size = carried_state.shape
    squares = jnp.sum(share_wide * share_wide, axis=1, keepdims=True)
    coarse = squares.astype(jnp.bfloat16)
    rest = (squares - coarse.astype(jnp.float32)).astype(jnp.bfloat16)
    lanes = jnp.concatenate([coarse, rest, jnp.zeros((coarse.shape[0], 126), jnp.bfloat16)], axis=1)
    projected = lax.psum_scatter(
        jnp.concatenate(
            [
                jnp.dot(mix_scaled, weight_part, preferred_element_type=jnp.float32).astype(
                    jnp.bfloat16
                )
                for weight_part in (query_weight, forget_weight, input_weight, outgate_weight)
            ]
            + [lanes],
            axis=1,
        ),
        ("kv", "tp"),
        scatter_dimension=0,
        tiled=True,
    ).astype(jnp.float32)
    own_squares = projected[:, -128:-127] + projected[:, -127:-126]
    projected = projected[:, :-128] * lax.rsqrt(own_squares / full_width + epsilon)
    key_width = head_count * key_size
    value_width = head_count * value_size
    query_act = projected[:, :key_width].reshape(state_rows, head_count, key_size)
    forget_pre = projected[:, key_width : 2 * key_width].reshape(state_rows, head_count, key_size)
    input_val = projected[:, 2 * key_width : 2 * key_width + value_width].reshape(
        state_rows, head_count, value_size
    )
    gate_pre = projected[:, 2 * key_width + value_width :].reshape(
        state_rows, head_count, value_size
    )
    floor_grid = forget_floor.reshape(head_count, key_size)
    forget = floor_grid + (1.0 - floor_grid) * jax.nn.sigmoid(forget_pre)
    next_state = (
        forget[..., None] * carried_state + (1.0 - forget)[..., None] * input_val[:, :, None, :]
    )
    readout = jnp.sum(next_state * jax.nn.silu(query_act)[..., None], axis=2)
    normed = (
        readout
        * lax.rsqrt(jnp.mean(readout * readout, axis=-1, keepdims=True) + epsilon)
        * head_gain
    )
    mixer_out = (
        (normed * jax.nn.silu(gate_pre)).reshape(state_rows, value_width).astype(jnp.bfloat16)
    )
    update = jnp.dot(
        gather_rows(mixer_out, chips, 1).reshape(state_rows * group_size, value_width),
        output_weight,
        preferred_element_type=jnp.float32,
    )
    middle = (share_wide + update).astype(jnp.bfloat16)
    layer_out = feed_forward(middle, second_gain, second_gate, second_up, second_down, chips, 2)
    return (layer_out, next_state)


def solution(mesh):
    in_specs = (
        P("dp", ("kv", "tp")),
        P(("dp", "kv", "tp"), None, None, None),
        P(),
        P(None, ("kv", "tp")),
        P(None, ("kv", "tp")),
        P(("kv", "tp"), None),
        P(),
        P(("kv", "tp"), None),
        P(("kv", "tp"), None),
        P(("kv", "tp"), None),
        P(("kv", "tp"), None),
        P(),
        P(),
        P(None, ("kv", "tp")),
        P(),
        P(None, ("kv", "tp")),
        P(None, ("kv", "tp")),
        P(("kv", "tp"), None),
    )
    out_specs = (P("dp", ("kv", "tp")), P(("dp", "kv", "tp"), None, None, None))
    return jax.shard_map(
        per_device, mesh=mesh, in_specs=in_specs, out_specs=out_specs, check_vma=False
    )
```

time: 344 us -> 261 us (0.76)
  waiting for transfers between devices: 202 us -> 55 us
  Pallas kernels: 0 us -> 128 us
  matrix products: 59.4 us -> 8.88 us
  blocking collectives: 14.5 us -> 0 us
  other arithmetic: 52.1 us -> 39.4 us
  local copies, waits for them, and re-layouts: 1.81 us -> 14.2 us
    pallas_call x0 -> x3, Pallas kernels: none -> 128 us  [the longest x2 111 us: feed_forward(): pl.pallas_call(functools.partial(block_kernel, chips), out_shape=jax.Shap...]
    reduce_scatter x2 -> x0, waiting for transfers between devices: 84.2 us -> none  [the longest x1 48.7 us: per_device(): lax.psum_scatter(first_terms, ('kv', 'tp'), scatter_dimension=1, tiled=True)]
    all_gather x3 -> x0, waiting for transfers between devices: 83.2 us -> none  [the longest x1 33.5 us: per_device(): lax.all_gather(tokens, ('kv', 'tp'), axis=1, tiled=True)]
    dot_general x5 -> x1, matrix products: 56.6 us -> 3.33 us  [per_device(): jnp.dot(gather_rows(mixer_out, chips, 1).reshape(state_rows * group_size,...]
    reduce_scatter x1, waiting for transfers between devices: 33.5 us -> 55 us  [per_device(): lax.psum_scatter(jnp.concatenate([jnp.dot(mix_scaled, weight_part, prefer...]
    psum x1 -> x0, blocking collectives: 14.5 us -> none  [per_device(): squares = lax.psum(jnp.sum(widened * widened, axis=1), ('kv', 'tp'))]
    concatenate x0 -> x1, local copies, waits for them, and re-layouts: none -> 7.39 us  [per_device(): jnp.concatenate([jnp.dot(mix_scaled, weight_part, preferred_element_type=...]
    reduce_sum x3 -> x1, other arithmetic: 5.48 us -> 1.14 us  [per_device(): squares = jnp.sum(share_wide * share_wide, axis=1, keepdims=True)]
  transfers between devices with their start and end apart: 6 -> 1, of which waited for: 6 -> 1; matrix products, arithmetic and copies ran while one was open for 0% -> 0% of each run, Pallas kernels for 0% -> 0%
where the time goes in v1:
time: 261 us; the launch traced here: 259 us
  Pallas kernels  128 us (49%)
  waiting for transfers between devices  55 us (21%)
  other arithmetic  39.4 us (15%)
  between operations  14.3 us (5%)
  local copies, waits for them, and re-layouts  14.2 us (5%)
  matrix products  8.88 us (3%)
    pallas_call x2, Pallas kernels, feed_forward(): pl.pallas_call(functools.partial(block_kernel, chips), out_shape=jax.Shap...  111 us
    reduce_scatter x1, waiting for transfers between devices, per_device(): lax.psum_scatter(jnp.concatenate([jnp.dot(mix_scaled, weight_part, prefer...  55 us
    reduce_sum x1, other arithmetic, per_device(): readout = jnp.sum(next_state * jax.nn.silu(query_act)[..., None], axis=2)  34.1 us
    pallas_call x1, Pallas kernels, gather_rows(): pl.pallas_call(functools.partial(gather_kernel, chips), out_shape=jax.Sha...  16.7 us
    concatenate x1, local copies, waits for them, and re-layouts, per_device(): jnp.concatenate([jnp.dot(mix_scaled, weight_part, preferred_element_type=...  7.39 us
    dot_general x4, matrix products, per_device(): jnp.dot(mix_scaled, weight_part, preferred_element_type=jnp.float32)  5.54 us
  transfers between devices with their start and end apart: 1, of which 1 were waited for; matrix products, arithmetic and copies ran while one was open for 0% of the time, Pallas kernels for 0%

profile of v1, /device:TPU:0, one launch (start us, length us, event | category | flops | bytes accessed | tf_op | source)
XLA Modules:
  0.0 259.5 jit_solution(5925075269664151837)
XLA Ops:
  7.2 0.0 copy-start
  7.2 0.0 reduce-scatter.2.cloned.1.call-start
  7.2 56.6 %shard_map.185 = bf16[256,512]{1,0:T(8,128)(2,1)} custom-call(bf16[256,512]{1,0:T(8,128)(2,1)} %own_ref.1, f32[8,1,512]{2,1,0:T(1,128)} %bitcast.48, bf16[4096,1408]{1,0:T(8,128)(2,1)} %gate_hbm.2, bf16[4096,1408]{1,0:T(8,128)(2,1)} %up_hbm.2, bf16[1408,4096]{1,0:T(8,128)(2,1)} %down_hbm.2), custom_call_target="tpu_custom_call" | custom-call | tf_op jit(solution)/shard_map/pallas_call | solution.py:285
  63.8 1.1 fusion.2
  65.0 0.1 copy.22
  65.2 0.9 dynamic_slice.3
  66.1 2.4 convolution_convert_fusion
  68.5 0.7 convolution_convert_fusion.1
  69.2 0.9 copy-done.4
  70.1 0.7 convolution_convert_fusion.2
  70.8 0.9 copy-done.5
  71.7 1.7 convolution_convert_fusion.3
  73.4 0.8 copy.23
  74.2 0.7 copy.24
  74.9 1.5 subtract_convert_fusion
  76.5 7.4 %concatenate.3 = bf16[256,8320]{1,0:T(8,128)(2,1)} concatenate(bf16[256,2048]{1,0:T(8,128)(2,1)} %convolution_convert_fusion.3, bf16[256,2048]{1,0:T(8,128)(2,1)S(1)} %convolution_convert_fusion.2, bf16[256,2048]{1,0:T(8,128)(2,1)S(1)} %convolution_convert_fusion.1, bf16[256,2048]{1,0:T(8,128)(2,1)S(1)} %convolution_convert_fusion, bf16[256,1]{1,0:T(8,128)(2,1)} %copy.24, ...), dimensions={1} | concatenate | bytes 8519680 | tf_op jit(solution)/shard_map/concatenate | solution.py:358
  83.9 0.0 reduce-scatter.2.cloned.1.call-update
  83.9 0.7 copy-done.6
  84.6 55.0 %reduce-scatter.2.cloned.1.call-done = bf16[32,8320]{1,0:T(8,128)(2,1)} async-done(((bf16[256,8320]{1,0:T(8,128)(2,1)}), bf16[32,8320]{1,0:T(8,128)(2,1)}) %reduce-scatter.2.cloned.1.call-update) | async-done | bytes 532496 | tf_op jit(solution)/shard_map/reduce_scatter | solution.py:357
  139.6 1.1 convert_element_type.73
  140.7 0.2 fusion.20
  140.9 0.1 slice_multiply_fusion
  141.1 0.1 fusion.12
  141.3 0.1 broadcast_subtract_fusion
  141.4 34.1 %multiply_reduce_fusion = (f32[32,16,128]{2,1,0:T(8,128)S(1)}, f32[32,16,128,128]{3,2,1,0:T(8,128)}) fusion(f32[32,16,128]{2,1,0:T(8,128)S(1)} %get-tuple-element.9, f32[32,16,128]{2,1,0:T(8,128)S(1)} %bitcast.44, f32[32,16,128]{2,1,0:T(8,128)S(1)} %get-tuple-element.4, f32[32,16,128,128]{3,2,1,0:T(8,128)} %param.19, f32[32,16,128]{2,1,0:T(8,128)S(1)} %get-tuple-element.5), kind=kLoop, calls=%fused_computation | loop fusion | flops 41877504 | bytes 68419584 | tf_op jit(solution)/shard_map/reduce_sum | solution.py:389
  175.5 0.1 multiply_reduce_fusion.1
  175.6 0.1 broadcast_multiply_fusion
  175.8 0.8 fusion.4.own_ref
  176.6 16.7 %shard_map.186 = bf16[8,32,2048]{2,1,0:T(8,128)(2,1)} custom-call(bf16[32,2048]{1,0:T(8,128)(2,1)} %fusion.4.own_ref), custom_call_target="tpu_custom_call" | custom-call | tf_op jit(solution)/shard_map/pallas_call | solution.py:81
  193.3 3.3 %fusion.own_ref = bf16[256,512]{1,0:T(8,128)(2,1)} fusion(bf16[256,2048]{1,0:T(8,128)(2,1)} %bitcast.45, bf16[2048,512]{1,0:T(8,128)(2,1)} %param.31, bf16[256,512]{1,0:T(8,128)(2,1)S(1)} %copy-done.2), kind=kOutput, calls=%fused_computation.7 | convolution fusion | flops 537264128 | bytes 3670016 | tf_op jit(solution)/shard_map/dot_general | solution.py:398
  196.6 54.4 %shard_map.187 = bf16[256,512]{1,0:T(8,128)(2,1)} custom-call(bf16[256,512]{1,0:T(8,128)(2,1)} %fusion.own_ref, f32[8,1,512]{2,1,0:T(1,128)} %bitcast.49, bf16[4096,1408]{1,0:T(8,128)(2,1)} %gate_hbm.3, bf16[4096,1408]{1,0:T(8,128)(2,1)} %up_hbm.3, bf16[1408,4096]{1,0:T(8,128)(2,1)} %down_hbm.3), custom_call_target="tpu_custom_call" | custom-call | tf_op jit(solution)/shard_map/pallas_call | solution.py:285
  251.0 1.7 copy.31
  (19 shorter events, 0.2 us)
Async XLA Ops:
  7.2 76.8 %copy-start = (f32[128]{0:T(128)S(1)}, f32[128]{0:T(128)}, u32[]{:S(2)}) copy-start(f32[128]{0:T(128)} %param.30) | copy-start | bytes 1540
  7.2 132.4 %reduce-scatter.2.cloned.1.call-start = ((), (), s32[]{:S(2)}) async-start(), calls=%async_computation.1 | async-start | bytes 4792320 | tf_op jit(solution)/shard_map/reduce_scatter | solution.py:357
  63.8 4.7 %copy-start.2 = (bf16[256,512]{1,0:T(8,128)(2,1)S(1)}, bf16[256,512]{1,0:T(8,128)(2,1)}, u32[]{:S(2)}) copy-start(bf16[256,512]{1,0:T(8,128)(2,1)} %shard_map.185) | copy-start | bytes 786436
  65.1 3.3 %copy-start.3 = (bf16[512,2048]{1,0:T(8,128)(2,1)S(1)}, bf16[512,2048]{1,0:T(8,128)(2,1)}, u32[]{:S(2)}) copy-start(bf16[512,2048]{1,0:T(8,128)(2,1)} %param.27) | copy-start | bytes 6291460
  68.5 1.6 copy-start.4
  70.1 1.6 copy-start.5
  83.9 0.7 copy-start.6
  196.6 56.0 %copy-start.1 = (f32[128]{0:T(128)S(1)}, f32[128]{0:T(128)}, u32[]{:S(2)}) copy-start(f32[128]{0:T(128)} %param.30) | copy-start | bytes 1540
Sparse Core Ops, SparseCore 0:
  84.0 55.5 reduce-scatter.1

commit v2 on v1

--- a/solution.py
+++ b/solution.py
@@ -319,6 +319,46 @@
     )(own, gain.reshape(blocks, 1, width), gate, up, down)
 
 
+def state_kernel(old_ref, forget_ref, query_ref, value_ref, new_ref, readout_ref):
+    batch, heads = old_ref.shape[:2]
+    for s in range(batch):
+        for h in range(heads):
+            value = value_ref[s, h : h + 1, :]
+            new = value + forget_ref[s, :, h : h + 1] * (old_ref[s, h] - value)
+            new_ref[s, h] = new
+            readout_ref[s, h : h + 1, :] = jnp.sum(
+                new * query_ref[s, :, h : h + 1], axis=0, keepdims=True
+            )
+
+
+def update_state(carried, forget, query, value):
+    rows, heads, keys, values = carried.shape
+    batch = 2 if rows % 2 == 0 else 1
+    cells = rows * heads * keys * values
+    return pl.pallas_call(
+        state_kernel,
+        grid=(rows // batch,),
+        out_shape=(
+            jax.ShapeDtypeStruct(carried.shape, jnp.float32),
+            jax.ShapeDtypeStruct((rows, heads, values), jnp.float32),
+        ),
+        in_specs=[
+            pl.BlockSpec((batch, heads, keys, values), lambda i: (i, 0, 0, 0)),
+            pl.BlockSpec((batch, keys, heads), lambda i: (i, 0, 0)),
+            pl.BlockSpec((batch, keys, heads), lambda i: (i, 0, 0)),
+            pl.BlockSpec((batch, heads, values), lambda i: (i, 0, 0)),
+        ],
+        out_specs=(
+            pl.BlockSpec((batch, heads, keys, values), lambda i: (i, 0, 0, 0)),
+            pl.BlockSpec((batch, heads, values), lambda i: (i, 0, 0)),
+        ),
+        compiler_params=pltpu.CompilerParams(vmem_limit_bytes=32 * 1024 * 1024),
+        cost_estimate=pl.CostEstimate(
+            flops=5 * cells, bytes_accessed=8 * cells, transcendentals=0
+        ),
+    )(carried, forget.swapaxes(1, 2), query.swapaxes(1, 2), value)
+
+
 def per_device(
     tokens,
     carried_state,
@@ -350,27 +390,24 @@
         share_wide * lax.dynamic_slice_in_dim(mix_gain, own_index * share_cols, share_cols)
     ).astype(jnp.bfloat16)
     state_rows, head_count, key_size, value_size = carried_state.shape
-    squares = jnp.sum(share_wide * share_wide, axis=1, keepdims=True)
-    coarse = squares.astype(jnp.bfloat16)
-    rest = (squares - coarse.astype(jnp.float32)).astype(jnp.bfloat16)
-    lanes = jnp.concatenate([coarse, rest, jnp.zeros((coarse.shape[0], 126), jnp.bfloat16)], axis=1)
+    squares = jnp.sum(share_wide * share_wide, axis=1).reshape(-1, 128)
+    lines = squares.shape[0]
+    padded = jnp.pad(squares, ((0, -lines % 8), (0, 0)))
+    squares = jnp.sum(gather_rows(padded, chips, 3), axis=0)[:lines].reshape(-1)
     projected = lax.psum_scatter(
         jnp.concatenate(
             [
-                jnp.dot(mix_scaled, weight_part, preferred_element_type=jnp.float32).astype(
-                    jnp.bfloat16
-                )
+                jnp.dot(mix_scaled, weight_part, preferred_element_type=jnp.float32)
                 for weight_part in (query_weight, forget_weight, input_weight, outgate_weight)
-            ]
-            + [lanes],
+            ],
             axis=1,
-        ),
+        ).astype(jnp.bfloat16),
         ("kv", "tp"),
         scatter_dimension=0,
         tiled=True,
     ).astype(jnp.float32)
-    own_squares = projected[:, -128:-127] + projected[:, -127:-126]
-    projected = projected[:, :-128] * lax.rsqrt(own_squares / full_width + epsilon)
+    own_squares = lax.dynamic_slice_in_dim(squares, own_index * state_rows, state_rows)
+    projected = projected * lax.rsqrt(own_squares / full_width + epsilon)[:, None]
     key_width = head_count * key_size
     value_width = head_count * value_size
     query_act = projected[:, :key_width].reshape(state_rows, head_count, key_size)
@@ -383,10 +420,7 @@
     )
     floor_grid = forget_floor.reshape(head_count, key_size)
     forget = floor_grid + (1.0 - floor_grid) * jax.nn.sigmoid(forget_pre)
-    next_state = (
-        forget[..., None] * carried_state + (1.0 - forget)[..., None] * input_val[:, :, None, :]
-    )
-    readout = jnp.sum(next_state * jax.nn.silu(query_act)[..., None], axis=2)
+    next_state, readout = update_state(carried_state, forget, jax.nn.silu(query_act), input_val)
     normed = (
         readout
         * lax.rsqrt(jnp.mean(readout * readout, axis=-1, keepdims=True) + epsilon)

time: 261 us -> 253 us (0.969)
  Pallas kernels: 128 us -> 172 us
  other arithmetic: 39.4 us -> 6.94 us
  waiting for transfers between devices: 55 us -> 40.8 us
  local copies, waits for them, and re-layouts: 14.2 us -> 9.09 us
    reduce_sum x2, other arithmetic: 35.2 us -> 0.9 us  [the longest x1 0.77 us: per_device(): squares = jnp.sum(gather_rows(padded, chips, 3), axis=0)[:lines].reshape(-1)]
    pallas_call x0 -> x1, Pallas kernels: none -> 33.2 us  [update_state(): pl.pallas_call(state_kernel, grid=(rows // batch,), out_shape=(jax.ShapeD...]
    reduce_scatter x1, waiting for transfers between devices: 55 us -> 40.8 us  [per_device(): lax.psum_scatter(jnp.concatenate([jnp.dot(mix_scaled, weight_part, prefer...]
    pallas_call x1 -> x2, Pallas kernels: 16.7 us -> 28.5 us  [gather_rows(): pl.pallas_call(functools.partial(gather_kernel, chips), out_shape=jax.Sha...]
    concatenate x1 -> x0, local copies, waits for them, and re-layouts: 7.39 us -> none  [per_device(): jnp.concatenate([jnp.dot(mix_scaled, weight_part, preferred_element_type=...]
    convert_element_type x4 -> x0, other arithmetic: 2.66 us -> none  [the longest x2 1.55 us: per_device(): rest = (squares - coarse.astype(jnp.float32)).astype(jnp.bfloat16)]
  transfers between devices with their start and end apart: 1 -> 1, of which waited for: 1 -> 1; matrix products, arithmetic and copies ran while one was open for 0% -> 1% of each run, Pallas kernels for 0% -> 5%
where the time goes in v2:
time: 253 us; the launch traced here: 251 us
  Pallas kernels  172 us (68%)
  waiting for transfers between devices  40.8 us (16%)
  between operations  14.2 us (6%)
  local copies, waits for them, and re-layouts  9.09 us (4%)
  matrix products  8 us (3%)
  other arithmetic  6.94 us (3%)
    pallas_call x2, Pallas kernels, feed_forward(): pl.pallas_call(functools.partial(block_kernel, chips), out_shape=jax.Shap...  111 us
    reduce_scatter x1, waiting for transfers between devices, per_device(): lax.psum_scatter(jnp.concatenate([jnp.dot(mix_scaled, weight_part, prefer...  40.8 us
    pallas_call x1, Pallas kernels, update_state(): pl.pallas_call(state_kernel, grid=(rows // batch,), out_shape=(jax.ShapeD...  33.2 us
    pallas_call x2, Pallas kernels, gather_rows(): pl.pallas_call(functools.partial(gather_kernel, chips), out_shape=jax.Sha...  28.5 us
  transfers between devices with their start and end apart: 1, of which 1 were waited for; matrix products, arithmetic and copies ran while one was open for 1% of the time, Pallas kernels for 5%

profile of v2, /device:TPU:0, one launch (start us, length us, event | category | flops | bytes accessed | tf_op | source)
XLA Modules:
  0.0 251.5 jit_solution(15689412751257035926)
XLA Ops:
  7.2 0.0 reduce-scatter.2.cloned.1.call-start
  7.2 0.8 dynamic_slice.6
  8.0 56.5 %shard_map.185 = bf16[256,512]{1,0:T(8,128)(2,1)} custom-call(bf16[256,512]{1,0:T(8,128)(2,1)} %own_ref.1, f32[8,1,512]{2,1,0:T(1,128)} %bitcast.55, bf16[4096,1408]{1,0:T(8,128)(2,1)} %gate_hbm.2, bf16[4096,1408]{1,0:T(8,128)(2,1)} %up_hbm.2, bf16[1408,4096]{1,0:T(8,128)(2,1)} %down_hbm.2), custom_call_target="tpu_custom_call" | custom-call | tf_op jit(solution)/shard_map/pallas_call | solution.py:285
  64.5 2.5 %convolution_convert_fusion.2 = bf16[256,2048]{1,0:T(8,128)(2,1)S(1)} fusion(bf16[512,2048]{1,0:T(8,128)(2,1)} %param.26, bf16[256,512]{1,0:T(8,128)(2,1)} %shard_map.185, f32[512]{0:T(512)S(1)} %dynamic_slice.6), kind=kOutput, calls=%fused_computation.3 | convolution fusion | flops 537788416 | bytes 3409920 | tf_op jit(solution)/shard_map/dot_general | solution.py:400
  67.0 0.7 convolution_convert_fusion.1
  67.8 0.9 copy-done.2
  68.6 0.7 convolution_convert_fusion
  69.4 0.9 copy-done.3
  70.2 0.7 convolution_convert_fusion.3
  70.9 2.2 pad_maximum_fusion
  73.2 0.7 copy-done.4
  73.9 0.1 copy.36
  74.0 0.1 copy.35
  74.1 0.1 fusion.2
  74.2 0.6 pad.4.own_ref
  74.8 11.7 %shard_map.186 = f32[8,8,128]{2,1,0:T(8,128)} custom-call(f32[8,128]{1,0:T(8,128)} %pad.4.own_ref), custom_call_target="tpu_custom_call" | custom-call | tf_op jit(solution)/shard_map/pallas_call | solution.py:81
  86.6 0.8 reduce_sum.28
  87.3 0.1 add_rsqrt_fusion.1
  87.4 40.8 %reduce-scatter.2.cloned.1.call-done = bf16[32,8192]{1,0:T(8,128)(2,1)} async-done(((bf16[256,8192]{1,0:T(8,128)(2,1)}), bf16[32,8192]{1,0:T(8,128)(2,1)}) %reduce-scatter.2.cloned.1.call-update) | async-done | bytes 524304 | tf_op jit(solution)/shard_map/reduce_scatter | solution.py:397
  128.2 1.2 convert_multiply_fusion
  129.4 0.1 slice_bitcast_fusion.1
  129.7 0.6 copy.37
  130.3 1.9 copy.41
  132.2 2.2 multiply_bitcast_fusion
  134.4 33.2 %shard_map.187 = (f32[32,16,128,128]{3,2,1,0:T(8,128)}, f32[32,16,128]{2,1,0:T(8,128)S(1)}) custom-call(f32[32,16,128,128]{3,2,1,0:T(8,128)} %old_ref.1, f32[32,128,16]{2,1,0:T(8,128)S(1)} %get-tuple-element.11.forget_ref, f32[32,128,16]{2,1,0:T(8,128)S(1)} %get-tuple-element.10.query_ref, f32[32,16,128]{2,1,0:T(8,128)S(1)} %bitcast.48), custom_call_target="tpu_custom_call" | custom-call | flops 41943040 | bytes 67108864 | tf_op jit(solution)/shard_map/pallas_call | solution.py:338
  167.6 0.1 multiply_reduce_fusion
  167.8 0.1 fusion.11
  167.9 0.7 copy.48
  168.6 16.7 %shard_map.188 = bf16[8,32,2048]{2,1,0:T(8,128)(2,1)} custom-call(bf16[32,2048]{1,0:T(8,128)(2,1)} %bitcast.52), custom_call_target="tpu_custom_call" | custom-call | tf_op jit(solution)/shard_map/pallas_call | solution.py:81
  185.4 3.3 %fusion.own_ref = bf16[256,512]{1,0:T(8,128)(2,1)} fusion(bf16[256,2048]{1,0:T(8,128)(2,1)} %bitcast.51, bf16[2048,512]{1,0:T(8,128)(2,1)} %param.31, bf16[256,512]{1,0:T(8,128)(2,1)S(1)} %copy-done), kind=kOutput, calls=%fused_computation.8 | convolution fusion | flops 537264128 | bytes 3670016 | tf_op jit(solution)/shard_map/dot_general | solution.py:432
  188.7 54.2 %shard_map.189 = bf16[256,512]{1,0:T(8,128)(2,1)} custom-call(bf16[256,512]{1,0:T(8,128)(2,1)} %fusion.own_ref, f32[8,1,512]{2,1,0:T(1,128)} %bitcast.56, bf16[4096,1408]{1,0:T(8,128)(2,1)} %gate_hbm.3, bf16[4096,1408]{1,0:T(8,128)(2,1)} %up_hbm.3, bf16[1408,4096]{1,0:T(8,128)(2,1)} %down_hbm.3), custom_call_target="tpu_custom_call" | custom-call | tf_op jit(solution)/shard_map/pallas_call | solution.py:285
  242.9 1.7 copy.50
  (17 shorter events, 0.3 us)
Async XLA Ops:
  7.2 121.0 %reduce-scatter.2.cloned.1.call-start = ((), (), s32[]{:S(2)}) async-start(), calls=%async_computation.1 | async-start | bytes 4718592 | tf_op jit(solution)/shard_map/reduce_scatter | solution.py:397
  64.5 2.6 %copy-start = (bf16[256,512]{1,0:T(8,128)(2,1)S(1)}, bf16[256,512]{1,0:T(8,128)(2,1)}, u32[]{:S(2)}) copy-start(bf16[256,512]{1,0:T(8,128)(2,1)} %shard_map.185) | copy-start | bytes 786436
  64.5 2.6 %copy-start.1 = (bf16[512,2048]{1,0:T(8,128)(2,1)S(1)}, bf16[512,2048]{1,0:T(8,128)(2,1)}, u32[]{:S(2)}) copy-start(bf16[512,2048]{1,0:T(8,128)(2,1)} %param.27) | copy-start | bytes 6291460
  67.0 1.6 copy-start.2
  68.6 1.6 copy-start.3
  73.2 0.7 copy-start.4
  134.4 33.4 %copy-start.5 = (f32[128]{0:T(128)S(1)}, f32[128]{0:T(128)}, u32[]{:S(2)}) copy-start(f32[128]{0:T(128)} %param.30) | copy-start | bytes 1540
Sparse Core Ops, SparseCore 0:
  73.3 54.8 reduce-scatter.1
